TPU v7x, 128 devices: a whole 4x4x4 slice. The times are simulated.
128 devices in a mesh: rep: 2 (over z_hi), fs: 32 (over z_lo, y, x), tp: 2 (over core).
Axes of the slice: x: 4, y: 4, z: 4 (z_hi: 2, z_lo: 2; z = z_hi * 2 + z_lo), core: 2. Of those that a mesh axis runs over, the one named last changes fastest.
Arguments:
- tokens: bfloat16 [65536, 2048], P(('rep', 'fs'), 'tp'), may hold values from -6 to 6
- attention_pre_gain: float32 [2048], replicated, may hold values from 0.1 to 1.9
- query_matrix: bfloat16 [2048, 512], P('fs', 'tp'), may hold values from -0.125 to 0.125
- key_matrix: bfloat16 [2048, 512], P('fs', 'tp'), may hold values from -0.125 to 0.125
- value_matrix: bfloat16 [2048, 1024], P('fs', 'tp'), may hold values from -0.125 to 0.125
- decay_first_weight: bfloat16 [2048, 16], replicated, may hold values from -0.125 to 0.125
- decay_second_weight: bfloat16 [16, 512], P(None, 'tp'), may hold values from -1.5 to 1.5
- decay_offset_bias: float32 [512], P('tp'), may hold values from 0 to 6
- extra_log_surge: float32 [65536, 2], P(('rep', 'fs'), 'tp'), may hold values from -0.7 to 0
- readout_head_gain: float32 [512], replicated, may hold values from 0.1 to 1.9
- output_matrix: bfloat16 [1024, 2048], P('tp', 'fs'), may hold values from -2.4375 to 2.4375
- attention_post_gain: float32 [2048], P('tp'), may hold values from 0.1 to 1.9
- feedforward_pre_gain: float32 [2048], replicated, may hold values from 0.1 to 1.9
- up_matrix: bfloat16 [2048, 4096], P('fs', 'tp'), may hold values from -0.125 to 0.125
- down_matrix: bfloat16 [4096, 2048], P('tp', 'fs'), may hold values from -1.21875 to 1.21875
- feedforward_post_gain: float32 [2048], P('tp'), may hold values from 0.1 to 1.9
Outputs:
- layer_out: bfloat16 [65536, 2048], P(('rep', 'fs'), 'tp')
All inputs are finite; a program needn't handle non-finite values.
Results may differ from a plain program's by a relative error of at most 0.017.
Values may be sent and summed in bfloat16 or wider, within the bound.
No kernel may reach another device: no remote copies, remote signals or barrier semaphores. Data moves between devices by JAX's collectives and lax.ppermute only.
A program may use at most 128 MiB of HBM per device.

v0:
```python
import jax
import jax.numpy as jnp
from jax import lax
from jax.sharding import Mesh
from jax.sharding import PartitionSpec as P

KEY_WIDTH = 256
DV = 512
BLOCK = 64
FS = ("fs_0", "fs_1", "fs_2")
REP_FS = ("rep", "fs_0", "fs_1", "fs_2")
EPS = 1e-06


def sent_together(arrays, axis, dim, along):
    both = jnp.concatenate(arrays, axis=along)
    filled, at, done = (lax.all_gather(both, axis, axis=dim, tiled=True), 0, [])
    for a in arrays:
        done.append(lax.slice_in_dim(filled, at, at + a.shape[along], axis=along))
        at += a.shape[along]
    return tuple(done)


def cut_along(array, dim, devices):
    lengths = array.shape
    tiles = array.reshape(*lengths[:dim], devices, lengths[dim] // devices, *lengths[dim + 1 :])
    return jnp.moveaxis(tiles, dim, 0)


def sum_at_owner(array, axis, dim):
    devices = lax.axis_size(axis)
    tiles = lax.all_to_all(cut_along(array, dim, devices), axis, 0, 0, tiled=True)
    return jnp.sum(tiles.astype(jnp.float32), axis=0)


def sent_to_all(array, axis):
    devices = lax.axis_size(axis)
    return lax.all_to_all(
        jnp.broadcast_to(array[None], (devices, *array.shape)), axis, 0, 0, tiled=True
    )


def taken_together(array, axis):
    everything = sent_to_all(array, axis)
    return jnp.sum(everything, axis=0)


def joined_along(tiles, dim):
    lengths = list(tiles.shape[1:])
    lengths[dim] *= tiles.shape[0]
    return jnp.moveaxis(tiles, 0, dim).reshape(lengths)


def stacked_from(array, axes, sequence):
    tiles = array
    for k in sequence:
        tiles = lax.all_gather(tiles, axes[k])
    done = sequence[::-1]
    back = [done.index(k) for k in range(len(axes))]
    tiles = tiles.transpose(*back, *range(len(axes), tiles.ndim))
    return tiles.reshape(-1, *array.shape)


def whole_of(array, axes, sequence, dim):
    return joined_along(stacked_from(array, axes, sequence), dim)


def pre_norm(rows, gain):
    values = rows.astype(jnp.float32)
    scale = lax.rsqrt(jnp.mean(values * values, axis=-1, keepdims=True) + EPS)
    return (values * scale * gain).astype(jnp.bfloat16)


def block_attention(queries, keys_in, values_in, log_gates):
    head_count, token_length, key_size = queries.shape
    value_size = values_in.shape[-1]
    blocks = token_length // BLOCK

    def to_blocks(array):
        return array.reshape(head_count, blocks, BLOCK, array.shape[-1]).transpose(1, 0, 2, 3)

    causal = jnp.tril(jnp.ones((BLOCK, BLOCK), dtype=bool))[None, :, :, None]
    highest = lax.Precision.HIGHEST

    def advance(memory_state, inputs):
        query_blk, key_blk, value_blk, gate_blk = inputs
        cumulative = jnp.cumsum(gate_blk, axis=1)
        carried = jnp.einsum(
            "hid,hde->hie", query_blk * jnp.exp(cumulative), memory_state, precision=highest
        )
        spread_log = cumulative[:, :, None, :] - cumulative[:, None, :, :]
        weights = jnp.exp(jnp.where(causal, spread_log, -jnp.inf))
        scores = jnp.einsum("hid,hjd,hijd->hij", query_blk, key_blk, weights, precision=highest)
        readout = carried + jnp.einsum("hij,hje->hie", scores, value_blk, precision=highest)
        final_log = cumulative[:, -1:, :]
        memory_state = jnp.exp(final_log[:, 0, :])[:, :, None] * memory_state + jnp.einsum(
            "hjd,hje->hde", key_blk * jnp.exp(final_log - cumulative), value_blk, precision=highest
        )
        return (memory_state, readout)

    start_state = jnp.zeros((head_count, key_size, value_size), jnp.float32)
    _, readout = lax.scan(
        advance,
        start_state,
        (to_blocks(queries), to_blocks(keys_in), to_blocks(values_in), to_blocks(log_gates)),
    )
    return readout.transpose(1, 0, 2, 3).reshape(head_count, token_length, value_size)


def make_adder(left):

    def add_rows(total, piece, start):
        return jnp.dot(left, piece, preferred_element_type=jnp.float32)

    return add_rows


def make_projector(left, piece):
    return jnp.dot(left, piece, preferred_element_type=jnp.float32)


def on_device(
    tokens,
    attention_pre_gain,
    query_matrix,
    key_matrix,
    value_matrix,
    decay_first_weight,
    decay_second_weight,
    decay_offset_bias,
    extra_log_surge,
    readout_head_gain,
    output_matrix,
    attention_post_gain,
    feedforward_pre_gain,
    up_matrix,
    down_matrix,
    feedforward_post_gain,
):
    token_length = tokens.shape[0]
    gathered = lax.all_gather(tokens, "tp", axis=1, tiled=True)
    width = gathered.shape[1]
    normed = pre_norm(gathered, attention_pre_gain)
    add_rows = make_adder(normed)
    key_cols = query_matrix.shape[1]
    value_cols = value_matrix.shape[1]
    empty_key = jnp.zeros((token_length, key_cols), jnp.float32)
    empty_value = jnp.zeros((token_length, value_cols), jnp.float32)
    pieces = sent_together((query_matrix, key_matrix, value_matrix), FS, 0, 1)
    start = jnp.int32(0)
    query_proj = add_rows(empty_key, pieces[0], start)
    key_proj = add_rows(empty_key, pieces[1], start)
    value_proj = add_rows(empty_value, pieces[2], start)
    query_proj = query_proj.astype(jnp.bfloat16)
    key_proj = key_proj.astype(jnp.bfloat16)
    value_proj = value_proj.astype(jnp.bfloat16)
    rank_rows = jnp.dot(normed, decay_first_weight, preferred_element_type=jnp.float32).astype(
        jnp.bfloat16
    )
    gate_source_input = (
        jnp.dot(rank_rows, decay_second_weight, preferred_element_type=jnp.float32)
        + decay_offset_bias
    )
    head_count = key_cols // KEY_WIDTH
    logarithm_decay = (jax.nn.log_sigmoid(gate_source_input) / 16.0).reshape(
        token_length, head_count, KEY_WIDTH
    ) + extra_log_surge[:, :, None]

    def by_head(array, size):
        return array.astype(jnp.float32).reshape(token_length, head_count, size).transpose(1, 0, 2)

    queries = by_head(query_proj, KEY_WIDTH) * KEY_WIDTH ** (-0.5)
    readout = block_attention(
        queries,
        by_head(key_proj, KEY_WIDTH),
        by_head(value_proj, DV),
        logarithm_decay.transpose(1, 0, 2),
    )
    readout = readout.transpose(1, 0, 2)
    head_scale = lax.rsqrt(jnp.mean(readout * readout, axis=-1, keepdims=True) + EPS)
    mixed = (
        (readout * head_scale * readout_head_gain)
        .astype(jnp.bfloat16)
        .reshape(token_length, value_cols)
    )
    partial_attn = make_projector(mixed, lax.all_gather(output_matrix, FS, axis=1, tiled=True))
    attn = sum_at_owner(partial_attn.astype(jnp.bfloat16), "tp", 1)
    attn_total = taken_together(jnp.sum(attn * attn, axis=1), "tp")
    attn_scale = lax.rsqrt(attn_total / width + EPS)[:, None]
    resid = (tokens.astype(jnp.float32) + attn * attn_scale * attention_post_gain).astype(
        jnp.bfloat16
    )
    gathered_mid = lax.all_gather(resid, "tp", axis=1, tiled=True)
    normed_mid = pre_norm(gathered_mid, feedforward_pre_gain)
    whole_up = whole_of(up_matrix, FS, (0, 1, 2), 0)
    hidden = jnp.dot(normed_mid, whole_up, preferred_element_type=jnp.float32)
    hidden = jax.nn.relu(hidden)
    squared = (hidden * hidden).astype(jnp.bfloat16)
    partial_feed = make_projector(squared, lax.all_gather(down_matrix, FS, axis=1, tiled=True))
    feed = sum_at_owner(partial_feed.astype(jnp.bfloat16), "tp", 1)
    feed_total = taken_together(jnp.sum(feed * feed, axis=1), "tp")
    feed_scale = lax.rsqrt(feed_total / width + EPS)[:, None]
    return (resid.astype(jnp.float32) + feed * feed_scale * feedforward_post_gain).astype(
        jnp.bfloat16
    )


def solution(mesh):
    finer = Mesh(
        mesh.devices.reshape(mesh.shape["rep"], 2, 4, 4, mesh.shape["tp"]),
        ("rep", "fs_0", "fs_1", "fs_2", "tp"),
    )
    in_specs = (
        P(REP_FS, "tp"),
        P(),
        P(FS, "tp"),
        P(FS, "tp"),
        P(FS, "tp"),
        P(),
        P(None, "tp"),
        P("tp"),
        P(REP_FS, "tp"),
        P(),
        P("tp", FS),
        P("tp"),
        P(),
        P(FS, "tp"),
        P("tp", FS),
        P("tp"),
    )
    out_specs = P(REP_FS, "tp")
    return jax.shard_map(
        on_device, mesh=finer, in_specs=in_specs, out_specs=out_specs, check_vma=False
    )
```

profile of v0, /device:TPU:1, one launch (start us, length us, event | category | flops | bytes accessed | tf_op | source)
XLA Modules:
  0.0 702.0 jit_solution(12112254873719032597)
XLA Ops:
  9.6 11.1 %all-gather = bf16[128,2048]{1,0:T(8,128)(2,1)} all-gather(bf16[64,2048]{1,0:T(8,128)(2,1)} %param.31), channel_id=2, replica_groups=mesh['rep'=2,'fs_0'=2,'fs_1'=4,'fs_2'=4,'tp'=2] {'fs_0'}, dimensions={0}, use_global_device_ids=true | all-gather | bytes 786432 | tf_op jit(solution)/shard_map/all_gather | solution.py:57
  20.8 8.2 %all-gather.11.cloned.1.call-done = bf16[1024,2048]{1,0:T(8,128)(2,1)} async-done(((bf16[1024,1024]{1,0:T(8,128)(2,1)}), bf16[1024,2048]{1,0:T(8,128)(2,1)}) %all-gather.11.cloned.1.call-update) | async-done | bytes 4194320 | tf_op jit(solution)/shard_map/all_gather | solution.py:141
  29.0 3.2 fusion.30
  32.5 3.0 fusion.32
  35.5 5.2 fusion.60
  40.7 127.3 %all-gather.13.cloned.1.call-done = bf16[2048,1024]{1,0:T(8,128)(2,1)} async-done(((bf16[64,1024]{1,0:T(8,128)(2,1)}), bf16[2048,1024]{1,0:T(8,128)(2,1)}) %all-gather.13.cloned.1.call-update) | async-done | bytes 4194320 | tf_op jit(solution)/shard_map/all_gather | solution.py:17
  168.0 5.3 fusion.52
  177.3 2.3 fusion.57
  179.6 150.9 %while.13 = (s32[]{:T(128)}, f32[1,256,512]{2,1,0:T(8,128)S(1)}, f32[16,1,64,512]{3,2,1,0:T(8,128)S(1)}, f32[16,1,64,256]{3,2,1,0:T(8,128)}, f32[16,1,64,256]{3,...) while((s32[]{:T(128)}, f32[1,256,512]{2,1,0:T(8,128)S(1)}, ...), condition=%wide.region_3.4_spmd.clone, body=%wide.region_1.3_spmd.clone.sunk | while | flops 233373696 | bytes 11649660 | solution.py:102
  182.3 2.5 fusion.94
  187.3 1.6 fusion.92
  191.7 2.5 fusion.94
  196.8 1.6 fusion.92
  201.1 2.5 fusion.94
  206.2 1.6 fusion.92
  210.6 2.5 fusion.94
  220.0 2.5 fusion.94
  225.1 1.6 fusion.92
  229.4 2.5 fusion.94
  238.9 2.5 fusion.94
  243.9 1.6 fusion.92
  248.3 2.5 fusion.94
  253.4 1.6 fusion.92
  257.7 2.5 fusion.94
  267.2 2.5 fusion.94
  276.6 2.5 fusion.94
  286.0 2.5 fusion.94
  295.5 2.5 fusion.94
  304.9 2.5 fusion.94
  314.3 2.5 fusion.94
  323.7 2.5 fusion.94
  328.8 1.6 fusion.92
  332.0 4.3 convolution_convert_fusion
  336.8 27.5 %all_to_all.22 = bf16[2,1024,1024]{2,1,0:T(8,128)(2,1)S(1)} all-to-all(bf16[2,1024,1024]{2,1,0:T(8,128)(2,1)S(1)} %bitcast.148), channel_id=1, replica_groups=mesh['rep'=2,'fs_0'=2,'fs_1'=4,'fs_2'=4,'tp'=2] {'tp'}, dimensions={0} | all-to-all | bytes 8388608 | tf_op jit(solution)/shard_map/all_to_all | solution.py:32
  365.4 1.9 copy-done.3
  367.7 3.9 all_to_all.23
  371.6 4.2 add_convert_fusion.1
  377.2 16.5 %all-gather.17.cloned.1.call-done = bf16[1024,2048]{1,0:T(8,128)(2,1)} async-done(((bf16[1024,1024]{1,0:T(8,128)(2,1)}), bf16[1024,2048]{1,0:T(8,128)(2,1)}) %all-gather.17.cloned.1.call-update) | async-done | bytes 4194320 | tf_op jit(solution)/shard_map/all_gather | solution.py:193
  393.7 3.1 fusion.33
  396.8 82.2 %all-gather.23.cloned.1.call-done = bf16[16,2,64,2048]{3,2,1,0:T(8,128)(2,1)} async-done(((bf16[4,2,64,2048]{3,2,1,0:T(8,128)(2,1)}), bf16[16,2,64,2048]{3,2,1,0:T(8,128)(2,1)}) %all-gather.23.cloned.1.call-update) | async-done | bytes 8388624 | tf_op jit(solution)/shard_map/all_gather | solution.py:57
  479.0 8.3 %copy.56 = bf16[2,4,4,64,2048]{4,3,2,1,0:T(8,128)(2,1)} copy(bf16[2,4,4,64,2048]{4,3,0,1,2:T(8,128)(2,1)} %bitcast.150) | data formatting | bytes 16777216 | tf_op jit(solution)/shard_map/transpose | solution.py:60
  487.3 140.4 %all-gather.19.cloned.1.call-done = bf16[2048,2048]{0,1:T(8,128)(2,1)} async-done(((bf16[2048,64]{0,1:T(8,128)(2,1)}), bf16[2048,2048]{0,1:T(8,128)(2,1)}) %all-gather.19.cloned.1.call-update) | async-done | bytes 8388624 | tf_op jit(solution)/shard_map/all_gather | solution.py:199
  627.7 25.6 %fusion.45 = bf16[1024,2048]{1,0:T(8,128)(2,1)} fusion(bf16[2048,2048]{0,1:T(8,128)(2,1)} %all-gather.19.cloned.1.call-done, bf16[2048,2048]{1,0:T(8,128)(2,1)} %bitcast.151, bf16[1024,2048]{1,0:T(8,128)(2,1)} %all-gather.17.cloned.1.call-done, f32[2048]{0:T(1024)S(1)} %copy-done.14, f32[1024]{0:T(1024)S(1)} %add_rsqrt_fusion.2), kind=kOutput, calls=%fused_computation.61 | convolution fusion | flops 17196646400 | bytes 25178112 | tf_op jit(solution)/shard_map/dot_general | solution.py:119
  653.3 2.6 copy.73
  655.9 27.7 %all_to_all.24 = bf16[2,1024,1024]{2,1,0:T(8,128)(2,1)S(1)} all-to-all(bf16[2,1024,1024]{2,1,0:T(8,128)(2,1)S(1)} %bitcast.149), channel_id=1, replica_groups=mesh['rep'=2,'fs_0'=2,'fs_1'=4,'fs_2'=4,'tp'=2] {'tp'}, dimensions={0} | all-to-all | bytes 8388608 | tf_op jit(solution)/shard_map/all_to_all | solution.py:32
  684.7 1.9 copy-done.2
  687.0 3.9 all_to_all.25
  690.9 4.2 add_convert_fusion
  (224 shorter events, 111.7 us)
Async XLA Ops:
  6.5 29.0 %copy-start = (bf16[2048,16]{0,1:T(8,128)(2,1)S(1)}, bf16[2048,16]{0,1:T(8,128)(2,1)}, u32[]{:S(2)}) copy-start(bf16[2048,16]{0,1:T(8,128)(2,1)} %param.23) | copy-start | bytes 196612
  6.5 25.7 %copy-start.8 = (f32[2048]{0:T(1024)S(1)}, f32[2048]{0:T(1024)}, u32[]{:S(2)}) copy-start(f32[2048]{0:T(1024)} %param.19) | copy-start | bytes 24580
  6.5 22.5 %all-gather.11.cloned.1.call-start = ((), (), s32[]{:S(2)}) async-start(), calls=%async_computation.4 | async-start | bytes 6291456 | tf_op jit(solution)/shard_map/all_gather | solution.py:141
  7.3 160.7 %all-gather.13.cloned.1.call-start = ((), (), s32[]{:S(2)}) async-start(), calls=%async_computation.5 | async-start | bytes 4325376 | tf_op jit(solution)/shard_map/all_gather | solution.py:17
  8.8 323.2 %all-gather.15.cloned.1.call-start = ((), (), s32[]{:S(2)}) async-start(), calls=%async_computation.6 | async-start | bytes 2162688 | tf_op jit(solution)/shard_map/all_gather | solution.py:186
  9.6 366.3 %all-gather.21.cloned.1.call-start = ((), (), s32[]{:S(2)}) async-start(), calls=%async_computation.9 | async-start | bytes 2621440 | tf_op jit(solution)/shard_map/all_gather | solution.py:57
  20.7 372.9 %all-gather.17.cloned.1.call-start = ((), (), s32[]{:S(2)}) async-start(), calls=%async_computation.7 | async-start | bytes 6291456 | tf_op jit(solution)/shard_map/all_gather | solution.py:193
  29.0 3.4 copy-start.5
  32.5 3.0 copy-start.13
  32.5 3.0 copy-start.15
  32.5 3.0 copy-start.16
  168.0 6.9 copy-start.7
  168.0 6.9 copy-start.12
  179.6 151.2 %copy-start.11 = (f32[512]{0:T(512)S(1)}, f32[512]{0:T(512)}, u32[]{:S(2)}) copy-start(f32[512]{0:T(512)} %param.27) | copy-start | bytes 6148
  365.4 1.9 copy-start.3
  367.3 4.3 copy-start.6
  367.3 4.3 copy-start.9
  375.8 103.2 %all-gather.23.cloned.1.call-start = ((), (), s32[]{:S(2)}) async-start(), calls=%async_computation.10 | async-start | bytes 10485760 | tf_op jit(solution)/shard_map/all_gather | solution.py:57
  376.4 251.3 %all-gather.19.cloned.1.call-start = ((), (), s32[]{:S(2)}) async-start(), calls=%async_computation.8 | async-start | bytes 8650752 | tf_op jit(solution)/shard_map/all_gather | solution.py:199
  479.0 148.7 %copy-start.14 = (f32[2048]{0:T(1024)S(1)}, f32[2048]{0:T(1024)}, u32[]{:S(2)}) copy-start(f32[2048]{0:T(1024)} %param.30) | copy-start | bytes 24580
  684.7 1.9 copy-start.2
  686.6 4.3 copy-start.4
  686.6 4.3 copy-start.10
  690.9 4.2 copy-start.1
Sparse Core Ops, SparseCore 0:
  9.0 19.9 all-gather.10
  30.7 137.2 all-gather.12
  169.6 151.2 all-gather.14
  322.4 52.6 all-gather.20
  376.7 16.9 all-gather.16
  395.2 83.7 all-gather.22
  480.7 147.0 all-gather.18
where the time goes:
time: 705 us; the launch traced here: 702 us
  waiting for transfers between devices  377 us (53%)
  matrix products  111 us (16%)
  other arithmetic  81.5 us (12%)
  blocking collectives  74 us (10%)
  local copies, waits for them, and re-layouts  43.6 us (6%)
  between operations  13.7 us (2%)
    all_gather x1, waiting for transfers between devices, on_device(): lax.all_gather(down_matrix, FS, axis=1, tiled=True)  140 us
    all_gather x1, waiting for transfers between devices, sent_together(): filled, at, done = (lax.all_gather(both, axis, axis=dim, tiled=True), 0, [])  127 us
    all_gather x2, waiting for transfers between devices, stacked_from(): tiles = lax.all_gather(tiles, axes[k])  82.3 us
    all_to_all x2, blocking collectives, sum_at_owner(): lax.all_to_all(cut_along(array, dim, devices), axis, 0, 0, tiled=True)  55.2 us
    dot_general x16, other arithmetic, advance(): jnp.einsum('hid,hjd,hijd->hij', query_blk, key_blk, weights, precision=hi...  40.2 us
    dot_general x2, matrix products, make_projector(): return jnp.dot(left, piece, preferred_element_type=jnp.float32)  29.9 us
    dot_general x16, matrix products, advance(): jnp.einsum('hjd,hje->hde', key_blk * jnp.exp(final_log - cumulative), val...  26.2 us
    dot_general x16, matrix products, advance(): jnp.einsum('hid,hde->hie', query_blk * jnp.exp(cumulative), memory_state,...  20.8 us
  transfers between devices with their start and end apart: 7, of which 5 were waited for; matrix products, arithmetic and copies ran while one was open for 28% of the time, Pallas kernels for 0%

commit v1 on v0

--- a/solution.py
+++ b/solution.py
@@ -196,7 +196,12 @@
     hidden = jnp.dot(normed_mid, whole_up, preferred_element_type=jnp.float32)
     hidden = jax.nn.relu(hidden)
     squared = (hidden * hidden).astype(jnp.bfloat16)
-    partial_feed = make_projector(squared, lax.all_gather(down_matrix, FS, axis=1, tiled=True))
+    partial_feed = make_projector(
+        squared,
+        jnp.concatenate(
+            lax.all_to_all(jnp.stack([down_matrix] * lax.axis_size(FS)), FS, 0, 0), axis=1
+        ),
+    )
     feed = sum_at_owner(partial_feed.astype(jnp.bfloat16), "tp", 1)
     feed_total = taken_together(jnp.sum(feed * feed, axis=1), "tp")
     feed_scale = lax.rsqrt(feed_total / width + EPS)[:, None]

time: 705 us -> 617 us (0.88)
  waiting for transfers between devices: 377 us -> 299 us
  blocking collectives: 74 us -> 53.4 us
    all_gather x1 -> x0, waiting for transfers between devices: 140 us -> none  [on_device(): lax.all_gather(down_matrix, FS, axis=1, tiled=True)]
    all_gather x2, waiting for transfers between devices: 82.3 us -> 155 us  [stacked_from(): tiles = lax.all_gather(tiles, axes[k])]
    all_to_all x2, blocking collectives: 55.2 us -> 34.6 us  [sum_at_owner(): lax.all_to_all(cut_along(array, dim, devices), axis, 0, 0, tiled=True)]
    all_gather x1, waiting for transfers between devices: 16.5 us -> 7.28 us  [on_device(): gathered_mid = lax.all_gather(resid, 'tp', axis=1, tiled=True)]
    another operation x16 -> x17, local copies, waits for them, and re-layouts: 14.2 us -> 18.5 us
  transfers between devices with their start and end apart: 7 -> 7, of which waited for: 5 -> 5; matrix products, arithmetic and copies ran while one was open for 28% -> 33% of each run, Pallas kernels for 0% -> 0%
where the time goes in v1:
time: 617 us; the launch traced here: 612 us
  waiting for transfers between devices  299 us (48%)
  matrix products  110 us (18%)
  other arithmetic  79.8 us (13%)
  blocking collectives  53.4 us (9%)
  local copies, waits for them, and re-layouts  48.1 us (8%)
  between operations  13.7 us (2%)
  starting transfers between devices  7.1 us (1%)
    all_gather x2, waiting for transfers between devices, stacked_from(): tiles = lax.all_gather(tiles, axes[k])  155 us
    all_gather x1, waiting for transfers between devices, sent_together(): filled, at, done = (lax.all_gather(both, axis, axis=dim, tiled=True), 0, [])  127 us
    dot_general x16, other arithmetic, advance(): jnp.einsum('hid,hjd,hijd->hij', query_blk, key_blk, weights, precision=hi...  38.5 us
    all_to_all x2, blocking collectives, sum_at_owner(): lax.all_to_all(cut_along(array, dim, devices), axis, 0, 0, tiled=True)  34.6 us
    dot_general x2, matrix products, make_projector(): return jnp.dot(left, piece, preferred_element_type=jnp.float32)  29.9 us
    dot_general x16, matrix products, advance(): jnp.einsum('hjd,hje->hde', key_blk * jnp.exp(final_log - cumulative), val...  26.2 us
    dot_general x16, matrix products, advance(): jnp.einsum('hid,hde->hie', query_blk * jnp.exp(cumulative), memory_state,...  20.8 us
    dot_general x16, matrix products, advance(): jnp.einsum('hij,hje->hie', scores, value_blk, precision=highest)  19.6 us
  transfers between devices with their start and end apart: 7, of which 5 were waited for; matrix products, arithmetic and copies ran while one was open for 33% of the time, Pallas kernels for 0%

profile of v1, /device:TPU:1, one launch (start us, length us, event | category | flops | bytes accessed | tf_op | source)
XLA Modules:
  0.0 612.0 jit_solution(17530343071921427471)
XLA Ops:
  9.6 11.1 %all-gather = bf16[128,2048]{1,0:T(8,128)(2,1)} all-gather(bf16[64,2048]{1,0:T(8,128)(2,1)} %param.31), channel_id=2, replica_groups=mesh['rep'=2,'fs_0'=2,'fs_1'=4,'fs_2'=4,'tp'=2] {'fs_0'}, dimensions={0}, use_global_device_ids=true | all-gather | bytes 786432 | tf_op jit(solution)/shard_map/all_gather | solution.py:57
  20.8 8.2 %all-gather.10.cloned.1.call-done = bf16[1024,2048]{1,0:T(8,128)(2,1)} async-done(((bf16[1024,1024]{1,0:T(8,128)(2,1)}), bf16[1024,2048]{1,0:T(8,128)(2,1)}) %all-gather.10.cloned.1.call-update) | async-done | bytes 4194320 | tf_op jit(solution)/shard_map/all_gather | solution.py:141
  29.0 3.2 fusion.30
  32.5 3.0 fusion.32
  35.5 5.2 fusion.60
  40.7 127.3 %all-gather.12.cloned.1.call-done = bf16[2048,1024]{1,0:T(8,128)(2,1)} async-done(((bf16[64,1024]{1,0:T(8,128)(2,1)}), bf16[2048,1024]{1,0:T(8,128)(2,1)}) %all-gather.12.cloned.1.call-update) | async-done | bytes 4194320 | tf_op jit(solution)/shard_map/all_gather | solution.py:17
  168.0 3.9 convolution_convert_fusion.2
  173.1 2.3 fusion.52
  177.1 2.2 fusion.57
  179.3 149.1 %while.13 = (s32[]{:T(128)}, f32[1,256,512]{2,1,0:T(8,128)S(1)}, f32[16,1,64,512]{3,2,1,0:T(8,128)S(1)}, f32[16,1,64,256]{3,2,1,0:T(8,128)}, f32[16,1,64,256]{3,...) while((s32[]{:T(128)}, f32[1,256,512]{2,1,0:T(8,128)S(1)}, ...), condition=%wide.region_3.4_spmd.clone, body=%wide.region_1.3_spmd.clone.sunk | while | flops 233373696 | bytes 11650182 | solution.py:102
  182.0 2.4 fusion.94
  191.3 2.4 fusion.94
  196.3 1.6 fusion.92
  200.6 2.4 fusion.94
  205.6 1.6 fusion.92
  210.0 2.4 fusion.94
  219.3 2.4 fusion.94
  228.6 2.4 fusion.94
  233.6 1.6 fusion.92
  237.9 2.4 fusion.94
  247.3 2.4 fusion.94
  256.6 2.4 fusion.94
  265.9 2.4 fusion.94
  270.8 1.6 fusion.92
  275.2 2.4 fusion.94
  280.2 1.6 fusion.92
  284.6 2.4 fusion.94
  293.9 2.4 fusion.94
  303.2 2.4 fusion.94
  312.5 2.4 fusion.94
  321.8 2.4 fusion.94
  330.0 4.3 convolution_convert_fusion
  334.8 27.4 %all_to_all.27 = bf16[2,1024,1024]{2,1,0:T(8,128)(2,1)S(1)} all-to-all(bf16[2,1024,1024]{2,1,0:T(8,128)(2,1)S(1)} %bitcast.151), channel_id=1, replica_groups=mesh['rep'=2,'fs_0'=2,'fs_1'=4,'fs_2'=4,'tp'=2] {'tp'}, dimensions={0} | all-to-all | bytes 8388608 | tf_op jit(solution)/shard_map/all_to_all | solution.py:32
  363.2 1.9 copy-done.3
  365.5 3.9 all_to_all.28
  369.4 4.2 add_convert_fusion.1
  375.2 4.3 stack.2
  379.5 6.9 %all-to-all-start.2 = ((bf16[32,2048,64]{1,2,0:T(8,128)(2,1)}), bf16[32,2048,64]{1,2,0:T(8,128)(2,1)}, u32[]{:S(2)}, u32[]{:S(2)}) async-start(bf16[32,2048,64]{1,2,0:T(8,128)(2,1)} %stack.2), calls=%async_computation.2 | async-start | bytes 16777216 | tf_op jit(solution)/shard_map/all_to_all | solution.py:202
  386.4 7.3 %all-gather.16.cloned.1.call-done = bf16[1024,2048]{1,0:T(8,128)(2,1)} async-done(((bf16[1024,1024]{1,0:T(8,128)(2,1)}), bf16[1024,2048]{1,0:T(8,128)(2,1)}) %all-gather.16.cloned.1.call-update) | async-done | bytes 4194320 | tf_op jit(solution)/shard_map/all_gather | solution.py:193
  393.7 3.1 fusion.33
  396.8 153.1 %all-gather.20.cloned.1.call-done = bf16[16,2,64,2048]{3,2,1,0:T(8,128)(2,1)} async-done(((bf16[4,2,64,2048]{3,2,1,0:T(8,128)(2,1)}), bf16[16,2,64,2048]{3,2,1,0:T(8,128)(2,1)}) %all-gather.20.cloned.1.call-update) | async-done | bytes 8388624 | tf_op jit(solution)/shard_map/all_gather | solution.py:57
  549.9 8.3 %copy.57 = bf16[2,4,4,64,2048]{4,3,2,1,0:T(8,128)(2,1)} copy(bf16[2,4,4,64,2048]{4,3,0,1,2:T(8,128)(2,1)} %bitcast.153) | data formatting | bytes 16777216 | tf_op jit(solution)/shard_map/transpose | solution.py:60
  558.2 25.6 %fusion.45 = bf16[1024,2048]{1,0:T(8,128)(2,1)} fusion(bf16[2048,2048]{0,1:T(8,128)(2,1)} %bitcast.18, bf16[2048,2048]{1,0:T(8,128)(2,1)} %bitcast.154, bf16[1024,2048]{1,0:T(8,128)(2,1)} %all-gather.16.cloned.1.call-done, f32[2048]{0:T(1024)S(1)} %copy-done.15, f32[1024]{0:T(1024)S(1)} %add_rsqrt_fusion.2), kind=kOutput, calls=%fused_computation.61 | convolution fusion | flops 17196646400 | bytes 25178112 | tf_op jit(solution)/shard_map/dot_general | solution.py:119
  583.8 2.6 copy.74
  586.4 7.2 %all_to_all.29 = bf16[2,1024,1024]{2,1,0:T(8,128)(2,1)S(1)} all-to-all(bf16[2,1024,1024]{2,1,0:T(8,128)(2,1)S(1)} %bitcast.152), channel_id=1, replica_groups=mesh['rep'=2,'fs_0'=2,'fs_1'=4,'fs_2'=4,'tp'=2] {'tp'}, dimensions={0} | all-to-all | bytes 8388608 | tf_op jit(solution)/shard_map/all_to_all | solution.py:32
  594.7 1.9 copy-done.2
  597.0 3.9 all_to_all.30
  601.0 4.2 add_convert_fusion
  (226 shorter events, 114.2 us)
Async XLA Ops:
  6.5 29.0 %copy-start = (bf16[2048,16]{0,1:T(8,128)(2,1)S(1)}, bf16[2048,16]{0,1:T(8,128)(2,1)}, u32[]{:S(2)}) copy-start(bf16[2048,16]{0,1:T(8,128)(2,1)} %param.23) | copy-start | bytes 196612
  6.5 25.7 %copy-start.9 = (f32[2048]{0:T(1024)S(1)}, f32[2048]{0:T(1024)}, u32[]{:S(2)}) copy-start(f32[2048]{0:T(1024)} %param.19) | copy-start | bytes 24580
  6.5 22.5 %all-gather.10.cloned.1.call-start = ((), (), s32[]{:S(2)}) async-start(), calls=%async_computation.5 | async-start | bytes 6291456 | tf_op jit(solution)/shard_map/all_gather | solution.py:141
  7.3 160.7 %all-gather.12.cloned.1.call-start = ((), (), s32[]{:S(2)}) async-start(), calls=%async_computation.6 | async-start | bytes 4325376 | tf_op jit(solution)/shard_map/all_gather | solution.py:17
  8.8 321.1 %all-gather.14.cloned.1.call-start = ((), (), s32[]{:S(2)}) async-start(), calls=%async_computation.7 | async-start | bytes 2162688 | tf_op jit(solution)/shard_map/all_gather | solution.py:186
  9.6 365.6 %all-gather.18.cloned.1.call-start = ((), (), s32[]{:S(2)}) async-start(), calls=%async_computation.9 | async-start | bytes 2621440 | tf_op jit(solution)/shard_map/all_gather | solution.py:57
  20.7 373.0 %all-gather.16.cloned.1.call-start = ((), (), s32[]{:S(2)}) async-start(), calls=%async_computation.8 | async-start | bytes 6291456 | tf_op jit(solution)/shard_map/all_gather | solution.py:193
  29.0 3.4 copy-start.5
  32.5 3.0 copy-start.14
  32.5 3.0 copy-start.16
  32.5 3.0 copy-start.17
  168.0 5.0 copy-start.7
  168.0 5.1 copy-start.13
  179.3 149.5 %copy-start.12 = (f32[512]{0:T(512)S(1)}, f32[512]{0:T(512)}, u32[]{:S(2)}) copy-start(f32[512]{0:T(512)} %param.27) | copy-start | bytes 6148
  363.2 1.9 copy-start.3
  365.1 4.3 copy-start.6
  365.1 4.3 copy-start.10
  373.7 1.6 copy-start.8
  373.7 176.2 %all-gather.20.cloned.1.call-start = ((), (), s32[]{:S(2)}) async-start(), calls=%async_computation.10 | async-start | bytes 10485760 | tf_op jit(solution)/shard_map/all_gather | solution.py:57
  379.5 178.7 %all-to-all-start.2 = ((bf16[32,2048,64]{1,2,0:T(8,128)(2,1)}), bf16[32,2048,64]{1,2,0:T(8,128)(2,1)}, u32[]{:S(2)}, u32[]{:S(2)}) async-start(bf16[32,2048,64]{1,2,0:T(8,128)(2,1)} %stack.2), calls=%async_computation.2 | async-start | bytes 16777216 | tf_op jit(solution)/shard_map/all_to_all | solution.py:202
  549.9 8.3 %copy-start.15 = (f32[2048]{0:T(1024)S(1)}, f32[2048]{0:T(1024)}, u32[]{:S(2)}) copy-start(f32[2048]{0:T(1024)} %param.30) | copy-start | bytes 24580
  594.7 1.9 copy-start.2
  596.7 4.3 copy-start.4
  596.7 4.3 copy-start.11
  600.9 4.2 copy-start.1
Sparse Core Ops, SparseCore 0:
  9.0 19.9 all-gather.9
  30.7 137.2 all-gather.11
  169.6 151.6 all-gather.13
  322.9 52.3 all-gather.17
  376.7 16.9 all-gather.15
  395.2 154.6 all-gather.19
